TPU v7x, 256 devices: a whole 4x4x8 slice. The times are simulated.
256 devices in a mesh: sp: 64 (over z, x, core), tp: 4 (over y).
Axes of the slice: x: 4, y: 4, z: 8, core: 2. Of those that a mesh axis runs over, the one named last changes fastest.
Arguments:
- conv_in: bfloat16 [49152, 1024], P('sp', 'tp'), may hold values from -6 to 6
- conv_pre: bfloat16 [49152, 1024], P('sp', 'tp'), may hold values from -6 to 6
- conv_post: bfloat16 [49152, 1024], P('sp', 'tp'), may hold values from -6 to 6
- taps: float32 [3, 1024], P(None, 'tp'), may hold values from -3 to 3
- out_proj: bfloat16 [1024, 2048], P('tp'), may hold values from -0.1875 to 0.1875
- stream: bfloat16 [49152, 2048], P(('sp', 'tp')), may hold values from -6 to 6
- norm_gain: float32 [2048], replicated, may hold values from 0.1 to 1.9
- routes: int32 [49152, 2], P(('sp', 'tp')), may hold values from 0 to 63, all different within a row; in each aligned block of 192 rows (0 to 191, 192 to 383, ...) at most 8 rows name the same one
- route_weight: float32 [49152, 2], P(('sp', 'tp')), may hold values from 0.1 to 1
- gate_w: bfloat16 [64, 2048, 2048], P('sp', None, 'tp'), may hold values from -0.52734375 to 0.52734375
- up_w: bfloat16 [64, 2048, 2048], P('sp', None, 'tp'), may hold values from -0.52734375 to 0.52734375
- down_w: bfloat16 [64, 2048, 2048], P('sp', 'tp'), may hold values from -0.013244629 to 0.013244629
Outputs:
- output: bfloat16 [49152, 2048], P(('sp', 'tp'))
Inputs may be any that keep to these rules, and one draw needn't show every extreme that they name: `routes`: each row names 2 different experts. In each aligned block of 192 rows no expert is named more than 8 times, a bound that some block reaches.
All inputs are finite; a program needn't handle non-finite values.
Results may differ from a plain program's by a relative error of at most 0.015.
Values may be sent and summed in bfloat16 or wider, within the bound.
A program may use at most 128 MiB of HBM per device.

v0:
```python
import jax
import jax.numpy as jnp
from jax import lax
from jax.sharding import PartitionSpec as P

EPSILON = 1e-05
LIMIT = 7.0
ALPHA = 1.702
CAP = 8


def with_halo(x, axis):
    count, length = (lax.axis_size(axis), x.shape[0])
    up = [(i, (i + 1) % count) for i in range(count - 1)]
    down = [(j, i) for i, j in up]
    before = lax.ppermute(x[length - 1 :], axis, up)
    after = lax.ppermute(x[:1], axis, down)
    return jnp.concatenate([before, x, after], axis=0)


def clamped_unit(gate_pre, up_pre):
    gated = jnp.minimum(gate_pre, LIMIT)
    upward = jnp.clip(up_pre, -LIMIT, LIMIT)
    return (upward + 1.0) * gated * jax.nn.sigmoid(ALPHA * gated)


def local(
    conv_in,
    conv_pre,
    conv_post,
    taps,
    out_proj,
    stream,
    norm_gain,
    routes,
    route_weight,
    gate_w,
    up_w,
    down_w,
):
    product = conv_pre.astype(jnp.float32) * conv_in.astype(jnp.float32)
    padded = with_halo(product.astype(jnp.bfloat16), "sp").astype(product.dtype)
    convolved = taps[0] * padded[:-2] + taps[1] * padded[1:-1] + taps[2] * padded[2:]
    mixed = (conv_post.astype(jnp.float32) * convolved).astype(jnp.bfloat16)
    own_rows, width = stream.shape
    part = jnp.dot(mixed, out_proj, preferred_element_type=jnp.float32).astype(jnp.bfloat16)
    part = part.reshape(lax.axis_size("tp"), own_rows, width)
    branch = lax.all_to_all(part, "tp", split_axis=0, concat_axis=0, tiled=True)
    branch = branch.astype(jnp.float32).sum(axis=0)
    resid = (stream.astype(jnp.float32) + branch).astype(jnp.bfloat16)
    resid_f = resid.astype(jnp.float32)
    scale = lax.rsqrt(jnp.mean(resid_f * resid_f, axis=-1, keepdims=True) + EPSILON)
    normed = (resid_f * scale * norm_gain).astype(jnp.bfloat16)
    experts = lax.axis_size("sp")
    top = routes.shape[1]
    flat = routes.reshape(-1)
    onehot = (flat[:, None] == jnp.arange(experts, dtype=jnp.int32)[None, :]).astype(jnp.bfloat16)
    entry = jnp.arange(own_rows * top, dtype=jnp.int32)
    earlier = (entry[None, :] < entry[:, None]).astype(jnp.bfloat16)
    counts = jnp.dot(earlier, onehot, preferred_element_type=jnp.float32)
    rank = jnp.sum(counts * onehot.astype(jnp.float32), axis=1).astype(jnp.int32)
    slots = experts * CAP
    target = (flat * CAP + rank).reshape(own_rows, top)
    ids = jnp.arange(slots, dtype=jnp.int32)[None, None, :]
    chosen = target[:, :, None] == ids
    pick = chosen.any(axis=1).astype(jnp.bfloat16)
    outgoing = lax.dot_general(
        pick, normed, (((0,), (0,)), ((), ())), preferred_element_type=jnp.float32
    ).astype(jnp.bfloat16)
    outgoing = outgoing.reshape(experts, CAP, width)
    done = []
    for k in range(2):
        group = outgoing[:, k * 4 : (k + 1) * 4]
        arrived = lax.all_to_all(group, "sp", split_axis=0, concat_axis=0, tiled=True)
        rows = lax.all_gather(arrived.reshape(-1, width), "tp", axis=0, tiled=True)
        gate_pre = jnp.dot(rows, gate_w[0], preferred_element_type=jnp.float32)
        up_pre = jnp.dot(rows, up_w[0], preferred_element_type=jnp.float32)
        active = clamped_unit(gate_pre, up_pre).astype(jnp.bfloat16)
        partial = jnp.dot(active, down_w[0], preferred_element_type=jnp.float32)
        summed = lax.psum_scatter(
            partial.astype(jnp.bfloat16), "tp", scatter_dimension=0, tiled=True
        )
        done.append(
            lax.all_to_all(
                summed.reshape(experts, 4, width), "sp", split_axis=0, concat_axis=0, tiled=True
            )
        )
    spread = jnp.sum(jnp.where(chosen, route_weight[:, :, None], 0.0), axis=1)
    total = resid.astype(jnp.float32)
    for k in range(2):
        share = spread.reshape(own_rows, experts, CAP)[:, :, k * 4 : (k + 1) * 4]
        share = share.reshape(own_rows, -1)
        high = share.astype(jnp.bfloat16)
        low = (share - high.astype(jnp.float32)).astype(jnp.bfloat16)
        back = done[k].reshape(-1, width)
        total = total + jnp.dot(high, back, preferred_element_type=jnp.float32)
        total = total + jnp.dot(low, back, preferred_element_type=jnp.float32)
    return total.astype(jnp.bfloat16)


def solution(mesh):
    placed = (
        P("sp", "tp"),
        P("sp", "tp"),
        P("sp", "tp"),
        P(None, "tp"),
        P("tp", None),
        P(("sp", "tp"), None),
        P(),
        P(("sp", "tp"), None),
        P(("sp", "tp"), None),
        P("sp", None, "tp"),
        P("sp", None, "tp"),
        P("sp", "tp", None),
    )
    return jax.shard_map(
        local, mesh=mesh, in_specs=placed, out_specs=P(("sp", "tp"), None), check_vma=False
    )
```

profile of v0, /device:TPU:1, one launch (start us, length us, event | category | flops | bytes accessed | tf_op | source)
XLA Modules:
  0.0 367.3 jit_solution(12065180576500988461)
XLA Ops:
  6.5 1.4 multiply_convert_fusion.2
  7.9 4.5 %collective-permute-start = (bf16[1,256]{1,0:T(2,128)(2,1)S(1)}, bf16[1,256]{1,0:T(2,128)(2,1)S(1)}, u32[]{:S(2)}, u32[]{:S(2)}) collective-permute-start(bf16[1,256]{1,0:T(2,128)(2,1)S(1)} %get-tuple-element.11), channel_id=1, source_target_pairs={{0,4},{4,8},{8,12},{12,16},{16,20},{20,24},{24,28},{28,32},{32,36}... | collective-permute-start | bytes 1544 | tf_op jit(solution)/shard_map/ppermute | solution.py:16
  12.4 1.9 collective-permute-start.1
  15.2 2.2 collective-permute-done.1
  17.4 2.8 convolution_convert_fusion.2
  20.2 4.8 %all-to-all-start = ((bf16[4,192,2048]{2,1,0:T(8,128)(2,1)}), bf16[4,192,2048]{2,1,0:T(8,128)(2,1)}, u32[]{:S(2)}, u32[]{:S(2)}) async-start(bf16[4,192,2048]{2,1,0:T(8,128)(2,1)} %bitcast.54), calls=%async_computation | async-start | bytes 6291456 | tf_op jit(solution)/shard_map/all_to_all | solution.py:48
  26.0 35.6 %all-to-all-done = bf16[4,192,2048]{2,1,0:T(8,128)(2,1)} async-done(((bf16[4,192,2048]{2,1,0:T(8,128)(2,1)}), bf16[4,192,2048]{2,1,0:T(8,128)(2,1)}, u32[]{:S(2)}, u32[]{:S(2)}) %all-to-all-start) | async-done | bytes 3145760 | tf_op jit(solution)/shard_map/all_to_all | solution.py:48
  61.6 2.7 convert_reduce_fusion
  66.3 2.1 fusion.54
  68.5 40.6 %all_to_all.25 = bf16[64,4,2048]{2,1,0:T(4,128)(2,1)S(1)} all-to-all(bf16[64,4,2048]{2,1,0:T(4,128)(2,1)S(1)} %get-tuple-element.8), channel_id=1, replica_groups=mesh['sp'=64,'tp'=4] {'sp'}, dimensions={0} | all-to-all | bytes 2097152 | tf_op jit(solution)/shard_map/all_to_all | solution.py:74
  109.1 1.2 reshape.55
  110.3 34.4 %all_to_all.26 = bf16[64,4,2048]{2,1,0:T(4,128)(2,1)S(1)} all-to-all(bf16[64,4,2048]{2,1,0:T(4,128)(2,1)} %get-tuple-element.7), channel_id=1, replica_groups=mesh['sp'=64,'tp'=4] {'sp'}, dimensions={0} | all-to-all | bytes 2097152 | tf_op jit(solution)/shard_map/all_to_all | solution.py:74
  144.8 1.1 reshape.53
  146.1 9.9 %all-gather.5.cloned.1.call-done = bf16[1024,2048]{1,0:T(8,128)(2,1)} async-done(((bf16[256,2048]{1,0:T(8,128)(2,1)}), bf16[1024,2048]{1,0:T(8,128)(2,1)}) %all-gather.5.cloned.1.call-update) | async-done | bytes 4194320 | tf_op jit(solution)/shard_map/all_gather | solution.py:75
  156.1 6.6 %fusion.12 = f32[1024,512]{1,0:T(8,128)} fusion(bf16[1024,2048]{1,0:T(8,128)(2,1)} %all-gather.5.cloned.1.call-done, bf16[1,2048,512]{2,1,0:T(8,128)(2,1)} %param.22), kind=kOutput, calls=%fused_computation.23 | convolution fusion | flops 2147483648 | bytes 8388608 | tf_op jit(solution)/shard_map/dot_general | solution.py:77
  162.7 10.3 %convolution_convert_fusion = bf16[1024,2048]{1,0:T(8,128)(2,1)} fusion(bf16[1,512,2048]{2,1,0:T(8,128)(2,1)S(1)} %copy-done, f32[1024,512]{1,0:T(8,128)} %fusion.12, bf16[1024,2048]{1,0:T(8,128)(2,1)} %all-gather.5.cloned.1.call-done, bf16[1,2048,512]{2,1,0:T(8,128)(2,1)} %param.21), kind=kOutput, calls=%fused_computation.1 | convolution fusion | flops 4302307328 | bytes 14680064 | tf_op jit(solution)/shard_map/dot_general | solution.py:79
  173.0 36.0 %all-gather.3.cloned.1.call-done = bf16[1024,2048]{1,0:T(8,128)(2,1)} async-done(((bf16[256,2048]{1,0:T(8,128)(2,1)}), bf16[1024,2048]{1,0:T(8,128)(2,1)}) %all-gather.3.cloned.1.call-update) | async-done | bytes 4194320 | tf_op jit(solution)/shard_map/all_gather | solution.py:75
  209.1 6.5 %fusion.14 = f32[1024,512]{1,0:T(8,128)} fusion(bf16[1024,2048]{1,0:T(8,128)(2,1)} %all-gather.3.cloned.1.call-done, bf16[1,2048,512]{2,1,0:T(8,128)(2,1)} %param.22), kind=kOutput, calls=%fused_computation.25 | convolution fusion | flops 2147483648 | bytes 8388608 | tf_op jit(solution)/shard_map/dot_general | solution.py:77
  215.6 10.3 %convolution_convert_fusion.1 = bf16[1024,2048]{1,0:T(8,128)(2,1)} fusion(bf16[1,512,2048]{2,1,0:T(8,128)(2,1)S(1)} %copy-done, f32[1024,512]{1,0:T(8,128)} %fusion.14, bf16[1024,2048]{1,0:T(8,128)(2,1)} %all-gather.3.cloned.1.call-done, bf16[1,2048,512]{2,1,0:T(8,128)(2,1)} %param.21), kind=kOutput, calls=%fused_computation.2 | convolution fusion | flops 4302307328 | bytes 14680064 | tf_op jit(solution)/shard_map/dot_general | solution.py:79
  225.9 35.6 %reduce-scatter.5.cloned.1.call-done = bf16[256,2048]{1,0:T(8,128)(2,1)} async-done(((bf16[1024,2048]{1,0:T(8,128)(2,1)}), bf16[256,2048]{1,0:T(8,128)(2,1)}) %reduce-scatter.5.cloned.1.call-update) | async-done | bytes 1048592 | tf_op jit(solution)/shard_map/reduce_scatter | solution.py:80
  261.5 2.2 reshape.56
  263.7 10.7 %all-to-all-start.4 = ((bf16[64,4,2048]{2,1,0:T(4,128)(2,1)}), bf16[64,4,2048]{2,1,0:T(4,128)(2,1)S(1)}, u32[]{:S(2)}, u32[]{:S(2)}) async-start(bf16[64,4,2048]{2,1,0:T(4,128)(2,1)} %reshape.56), calls=%async_computation.6 | async-start | bytes 2097152 | tf_op jit(solution)/shard_map/all_to_all | solution.py:84
  274.5 38.6 %reduce-scatter.3.cloned.1.call-done = bf16[256,2048]{1,0:T(8,128)(2,1)} async-done(((bf16[1024,2048]{1,0:T(8,128)(2,1)}), bf16[256,2048]{1,0:T(8,128)(2,1)}) %reduce-scatter.3.cloned.1.call-update) | async-done | bytes 1048592 | tf_op jit(solution)/shard_map/reduce_scatter | solution.py:80
  313.1 2.3 reshape.54
  316.4 10.7 %all-to-all-start.2 = ((bf16[64,4,2048]{2,1,0:T(4,128)(2,1)}), bf16[64,4,2048]{2,1,0:T(4,128)(2,1)S(1)}, u32[]{:S(2)}, u32[]{:S(2)}) async-start(bf16[64,4,2048]{2,1,0:T(4,128)(2,1)} %reshape.54), calls=%async_computation.3 | async-start | bytes 2097152 | tf_op jit(solution)/shard_map/all_to_all | solution.py:84
  327.3 1.0 copy.48
  328.3 1.4 fusion.55
  329.7 3.8 %convolution_bitcast_fusion.1 = f32[192,2048]{1,0:T(8,128)} fusion(bf16[64,4,2048]{2,1,0:T(4,128)(2,1)} %copy-done.1, f32[192,64,4]{0,2,1:T(4,128)S(1)} %get-tuple-element.10), kind=kOutput, calls=%fused_computation.7 | convolution fusion | flops 201326592 | bytes 2818048 | tf_op jit(solution)/shard_map/dot_general | solution.py:96
  333.5 2.5 convolution_bitcast_fusion
  336.0 19.3 %all-to-all-done.2 = bf16[64,4,2048]{2,1,0:T(4,128)(2,1)S(1)} async-done(((bf16[64,4,2048]{2,1,0:T(4,128)(2,1)}), bf16[64,4,2048]{2,1,0:T(4,128)(2,1)S(1)}, u32[]{:S(2)}, u32[]{:S(2)}) %all-to-all-start.2) | async-done | bytes 1048608 | tf_op jit(solution)/shard_map/all_to_all | solution.py:84
  355.3 1.4 convolution_bitcast_fusion.2
  356.9 3.9 %fusion.5 = bf16[192,2048]{1,0:T(8,128)(2,1)} fusion(f32[192,2048]{1,0:T(8,128)} %convolution_bitcast_fusion, f32[192,2048]{1,0:T(8,128)S(1)} %copy-done.5, f32[192,2048]{1,0:T(8,128)S(1)} %convolution_bitcast_fusion.2, bf16[192,2048]{1,0:T(8,128)(2,1)S(1)} %copy-done.4, bf16[64,4,2048]{2,1,0:T(4,128)(2,1)S(1)} %all-to-all-done.2, ...), kind=kOutput, calls=%fused_computation.14 | convolution fusion | flops 203685888 | bytes 7536640 | tf_op jit(solution)/shard_map/dot_general | solution.py:96
  (49 shorter events, 5.7 us)
Async XLA Ops:
  6.5 156.1 %copy-start = (bf16[1,512,2048]{2,1,0:T(8,128)(2,1)S(1)}, bf16[1,512,2048]{2,1,0:T(8,128)(2,1)}, u32[]{:S(2)}) copy-start(bf16[1,512,2048]{2,1,0:T(8,128)(2,1)} %param.23) | copy-start | bytes 6291460
  6.5 10.9 %copy-start.8 = (bf16[768,256]{1,0:T(8,128)(2,1)S(1)}, bf16[768,256]{1,0:T(8,128)(2,1)}, u32[]{:S(2)}) copy-start(bf16[768,256]{1,0:T(8,128)(2,1)} %param.14) | copy-start | bytes 1179652
  6.5 10.9 %copy-start.6 = (bf16[256,2048]{1,0:T(8,128)(2,1)S(1)}, bf16[256,2048]{1,0:T(8,128)(2,1)}, u32[]{:S(2)}) copy-start(bf16[256,2048]{1,0:T(8,128)(2,1)} %param.16) | copy-start | bytes 3145732
  7.9 7.2 %collective-permute-start = (bf16[1,256]{1,0:T(2,128)(2,1)S(1)}, bf16[1,256]{1,0:T(2,128)(2,1)S(1)}, u32[]{:S(2)}, u32[]{:S(2)}) collective-permute-start(bf16[1,256]{1,0:T(2,128)(2,1)S(1)} %get-tuple-element.11), channel_id=1, source_target_pairs={{0,4},{4,8},{8,12},{12,16},{16,20},{20,24},{24,28},{28,32},{32,36}... | collective-permute-start | bytes 1544 | tf_op jit(solution)/shard_map/ppermute | solution.py:16
  12.4 4.9 %collective-permute-start.1 = (bf16[1,256]{1,0:T(2,128)(2,1)S(1)}, bf16[1,256]{1,0:T(2,128)(2,1)S(1)}, u32[]{:S(2)}, u32[]{:S(2)}) collective-permute-start(bf16[1,256]{1,0:T(2,128)(2,1)S(1)} %get-tuple-element.12), channel_id=1, source_target_pairs={{4,0},{8,4},{12,8},{16,12},{20,16},{24,20},{28,24},{32,28},{36,32}... | collective-permute-start | bytes 1544 | tf_op jit(solution)/shard_map/ppermute | solution.py:17
  20.2 4.9 %copy-start.10 = (s32[192,2]{0,1:T(2,128)S(1)}, s32[192,2]{0,1:T(2,128)}, u32[]{:S(2)}) copy-start(s32[192,2]{0,1:T(2,128)} %param.19) | copy-start | bytes 4612
  20.2 41.3 %all-to-all-start = ((bf16[4,192,2048]{2,1,0:T(8,128)(2,1)}), bf16[4,192,2048]{2,1,0:T(8,128)(2,1)}, u32[]{:S(2)}, u32[]{:S(2)}) async-start(bf16[4,192,2048]{2,1,0:T(8,128)(2,1)} %bitcast.54), calls=%async_computation | async-start | bytes 6291456 | tf_op jit(solution)/shard_map/all_to_all | solution.py:48
  25.0 131.0 %all-gather.5.cloned.1.call-start = ((), (), s32[]{:S(2)}) async-start(), calls=%async_computation.9 | async-start | bytes 5242880 | tf_op jit(solution)/shard_map/all_gather | solution.py:75
  26.0 38.3 %copy-start.7 = (bf16[192,2048]{1,0:T(8,128)(2,1)S(1)}, bf16[192,2048]{1,0:T(8,128)(2,1)}, u32[]{:S(2)}) copy-start(bf16[192,2048]{1,0:T(8,128)(2,1)} %param.17) | copy-start | bytes 2359300
  64.3 1.2 copy-start.9
  64.6 0.9 copy-start.3
  110.3 98.8 %all-gather.3.cloned.1.call-start = ((), (), s32[]{:S(2)}) async-start(), calls=%async_computation.7 | async-start | bytes 5242880 | tf_op jit(solution)/shard_map/all_gather | solution.py:75
  145.9 115.6 %reduce-scatter.5.cloned.1.call-start = ((), (), s32[]{:S(2)}) async-start(), calls=%async_computation.10 | async-start | bytes 5242880 | tf_op jit(solution)/shard_map/reduce_scatter | solution.py:80
  173.0 140.1 %reduce-scatter.3.cloned.1.call-start = ((), (), s32[]{:S(2)}) async-start(), calls=%async_computation.8 | async-start | bytes 5242880 | tf_op jit(solution)/shard_map/reduce_scatter | solution.py:80
  263.7 51.6 %all-to-all-start.4 = ((bf16[64,4,2048]{2,1,0:T(4,128)(2,1)}), bf16[64,4,2048]{2,1,0:T(4,128)(2,1)S(1)}, u32[]{:S(2)}, u32[]{:S(2)}) async-start(bf16[64,4,2048]{2,1,0:T(4,128)(2,1)} %reshape.56), calls=%async_computation.6 | async-start | bytes 2097152 | tf_op jit(solution)/shard_map/all_to_all | solution.py:84
  274.5 52.6 %copy-start.11 = (f32[192,2]{0,1:T(2,128)S(1)}, f32[192,2]{0,1:T(2,128)}, u32[]{:S(2)}) copy-start(f32[192,2]{0,1:T(2,128)} %param.20) | copy-start | bytes 4612
  315.4 1.0 copy-start.1
  316.4 38.9 %all-to-all-start.2 = ((bf16[64,4,2048]{2,1,0:T(4,128)(2,1)}), bf16[64,4,2048]{2,1,0:T(4,128)(2,1)S(1)}, u32[]{:S(2)}, u32[]{:S(2)}) async-start(bf16[64,4,2048]{2,1,0:T(4,128)(2,1)} %reshape.54), calls=%async_computation.3 | async-start | bytes 2097152 | tf_op jit(solution)/shard_map/all_to_all | solution.py:84
  328.3 5.2 %copy-start.2 = (bf16[64,4,2048]{2,1,0:T(4,128)(2,1)S(1)}, bf16[64,4,2048]{2,1,0:T(4,128)(2,1)}, u32[]{:S(2)}) copy-start(bf16[64,4,2048]{2,1,0:T(4,128)(2,1)} %copy-done.1) | copy-start | bytes 3145732
  355.3 1.4 copy-start.4
  355.3 1.7 copy-start.5
Sparse Core Ops, SparseCore 0:
  110.4 45.6 all-gather.4
  157.9 51.1 all-gather.2
  211.6 49.8 reduce-scatter.4
  263.9 49.1 reduce-scatter.2
where the time goes:
time: 368 us; the launch traced here: 367 us
  waiting for transfers between devices  177 us (48%)
  blocking collectives  75 us (20%)
  matrix products  49.1 us (13%)
  starting transfers between devices  33 us (9%)
  local copies, waits for them, and re-layouts  14.8 us (4%)
  between operations  13.4 us (4%)
  other arithmetic  4.81 us (1%)
    all_to_all x2, blocking collectives, local(): lax.all_to_all(group, 'sp', split_axis=0, concat_axis=0, tiled=True)  75 us
    reduce_scatter x2, waiting for transfers between devices, local(): lax.psum_scatter(partial.astype(jnp.bfloat16), 'tp', scatter_dimension=0,...  74.2 us
    all_gather x2, waiting for transfers between devices, local(): rows = lax.all_gather(arrived.reshape(-1, width), 'tp', axis=0, tiled=True)  46 us
    all_to_all x1, waiting for transfers between devices, local(): branch = lax.all_to_all(part, 'tp', split_axis=0, concat_axis=0, tiled=True)  35.6 us
    all_to_all x2, starting transfers between devices, local(): lax.all_to_all(summed.reshape(experts, 4, width), 'sp', split_axis=0, con...  21.4 us
    dot_general x2, matrix products, local(): partial = jnp.dot(active, down_w[0], preferred_element_type=jnp.float32)  20.6 us
    all_to_all x2, waiting for transfers between devices, local(): lax.all_to_all(summed.reshape(experts, 4, width), 'sp', split_axis=0, con...  19.3 us
    dot_general x2, matrix products, local(): up_pre = jnp.dot(rows, up_w[0], preferred_element_type=jnp.float32)  13.1 us
  transfers between devices with their start and end apart: 9, of which 7 were waited for; matrix products, arithmetic and copies ran while one was open for 14% of the time, Pallas kernels for 0%

commit v1 on v0

--- a/solution.py
+++ b/solution.py
@@ -7,6 +7,25 @@
 LIMIT = 7.0
 ALPHA = 1.702
 CAP = 8
+
+
+def ring_gather(x, axis, dim):
+    size, here, span = (lax.axis_size(axis), lax.axis_index(axis), x.shape[dim])
+    right = [(i, (i + 1) % size) for i in range(size)]
+    backward = [(i, (i - 1) % size) for i in range(size)]
+    out = jnp.zeros((*x.shape[:dim], size * span, *x.shape[dim + 1 :]), x.dtype)
+    out = lax.dynamic_update_slice_in_dim(out, x, here * span, axis=dim)
+    from_left = from_right = x
+    halfway = size // 2
+    for step in range(1, halfway + 1):
+        from_left = lax.ppermute(from_left, axis, right)
+        out = lax.dynamic_update_slice_in_dim(out, from_left, (here - step) % size * span, axis=dim)
+        if step < size - halfway:
+            from_right = lax.ppermute(from_right, axis, backward)
+            out = lax.dynamic_update_slice_in_dim(
+                out, from_right, (here + step) % size * span, axis=dim
+            )
+    return out
 
 
 def with_halo(x, axis):
@@ -72,7 +91,7 @@
     for k in range(2):
         group = outgoing[:, k * 4 : (k + 1) * 4]
         arrived = lax.all_to_all(group, "sp", split_axis=0, concat_axis=0, tiled=True)
-        rows = lax.all_gather(arrived.reshape(-1, width), "tp", axis=0, tiled=True)
+        rows = ring_gather(arrived.reshape(-1, width), "tp", 0)
         gate_pre = jnp.dot(rows, gate_w[0], preferred_element_type=jnp.float32)
         up_pre = jnp.dot(rows, up_w[0], preferred_element_type=jnp.float32)
         active = clamped_unit(gate_pre, up_pre).astype(jnp.bfloat16)

time: 368 us -> 391 us (1.062)
  local copies, waits for them, and re-layouts: 14.8 us -> 25.9 us
  waiting for transfers between devices: 177 us -> 185 us
  starting transfers between devices: 33 us -> 39.5 us
  matrix products: 49.1 us -> 43.4 us
    ppermute x0 -> x6, waiting for transfers between devices: none -> 92.3 us  [the longest x4 92.3 us: ring_gather(): from_left = lax.ppermute(from_left, axis, right)]
    all_gather x2 -> x0, waiting for transfers between devices: 46 us -> none  [local(): rows = lax.all_gather(arrived.reshape(-1, width), 'tp', axis=0, tiled=True)]
    reduce_scatter x2, waiting for transfers between devices: 74.2 us -> 35.4 us  [local(): lax.psum_scatter(partial.astype(jnp.bfloat16), 'tp', scatter_dimension=0,...]
    dot_general x2, matrix products: 13.1 us -> 7.38 us  [local(): up_pre = jnp.dot(rows, up_w[0], preferred_element_type=jnp.float32)]
    ppermute x0 -> x6, starting transfers between devices: none -> 5.51 us  [the longest x2 5.13 us: ring_gather(): from_right = lax.ppermute(from_right, axis, backward)]
    unnamed x25 -> x35, local copies, waits for them, and re-layouts: 2.29 us -> 7.38 us
    dynamic_update_slice x0 -> x8, local copies, waits for them, and re-layouts: none -> 4.69 us  [the longest x4 2.86 us: ring_gather(): lax.dynamic_update_slice_in_dim(out, from_left, (here - step) % size * sp...]
  transfers between devices with their start and end apart: 9 -> 13, of which waited for: 7 -> 8; matrix products, arithmetic and copies ran while one was open for 14% -> 9% of each run, Pallas kernels for 0% -> 0%
where the time goes in v1:
time: 391 us; the launch traced here: 390 us
  waiting for transfers between devices  185 us (47%)
  blocking collectives  77.8 us (20%)
  matrix products  43.4 us (11%)
  starting transfers between devices  39.5 us (10%)
  local copies, waits for them, and re-layouts  25.9 us (7%)
  between operations  13.8 us (4%)
  other arithmetic  4.81 us (1%)
    ppermute x4, waiting for transfers between devices, ring_gather(): from_left = lax.ppermute(from_left, axis, right)  92.3 us
    all_to_all x2, blocking collectives, local(): lax.all_to_all(group, 'sp', split_axis=0, concat_axis=0, tiled=True)  77.8 us
    all_to_all x1, waiting for transfers between devices, local(): branch = lax.all_to_all(part, 'tp', split_axis=0, concat_axis=0, tiled=True)  35.6 us
    reduce_scatter x2, waiting for transfers between devices, local(): lax.psum_scatter(partial.astype(jnp.bfloat16), 'tp', scatter_dimension=0,...  35.4 us
    all_to_all x2, starting transfers between devices, local(): lax.all_to_all(summed.reshape(experts, 4, width), 'sp', split_axis=0, con...  22.7 us
    dot_general x2, matrix products, local(): partial = jnp.dot(active, down_w[0], preferred_element_type=jnp.float32)  20.6 us
    all_to_all x2, waiting for transfers between devices, local(): lax.all_to_all(summed.reshape(experts, 4, width), 'sp', split_axis=0, con...  19.3 us
  transfers between devices with their start and end apart: 13, of which 8 were waited for; matrix products, arithmetic and copies ran while one was open for 9% of the time, Pallas kernels for 0%

profile of v1, /device:TPU:1, one launch (start us, length us, event | category | flops | bytes accessed | tf_op | source)
XLA Modules:
  0.0 390.0 jit_solution(16133048525588361562)
XLA Ops:
  7.9 4.5 %collective-permute-start = (bf16[1,256]{1,0:T(2,128)(2,1)S(1)}, bf16[1,256]{1,0:T(2,128)(2,1)S(1)}, u32[]{:S(2)}, u32[]{:S(2)}) collective-permute-start(bf16[1,256]{1,0:T(2,128)(2,1)S(1)} %get-tuple-element.11), channel_id=1, source_target_pairs={{0,4},{4,8},{8,12},{12,16},{16,20},{20,24},{24,28},{28,32},{32,36}... | collective-permute-start | bytes 1544 | tf_op jit(solution)/shard_map/ppermute | solution.py:35
  12.4 1.9 collective-permute-start.1
  15.2 2.2 collective-permute-done.1
  17.4 2.8 convolution_convert_fusion.2
  20.2 4.8 %all-to-all-start = ((bf16[4,192,2048]{2,1,0:T(8,128)(2,1)}), bf16[4,192,2048]{2,1,0:T(8,128)(2,1)}, u32[]{:S(2)}, u32[]{:S(2)}) async-start(bf16[4,192,2048]{2,1,0:T(8,128)(2,1)} %bitcast.54), calls=%async_computation | async-start | bytes 6291456 | tf_op jit(solution)/shard_map/all_to_all | solution.py:67
  26.0 35.6 %all-to-all-done = bf16[4,192,2048]{2,1,0:T(8,128)(2,1)} async-done(((bf16[4,192,2048]{2,1,0:T(8,128)(2,1)}), bf16[4,192,2048]{2,1,0:T(8,128)(2,1)}, u32[]{:S(2)}, u32[]{:S(2)}) %all-to-all-start) | async-done | bytes 3145760 | tf_op jit(solution)/shard_map/all_to_all | solution.py:67
  61.5 2.7 convert_reduce_fusion
  66.3 2.1 fusion.54
  68.5 40.7 %all_to_all.25 = bf16[64,4,2048]{2,1,0:T(4,128)(2,1)} all-to-all(bf16[64,4,2048]{2,1,0:T(4,128)(2,1)S(1)} %get-tuple-element.8), channel_id=1, replica_groups=mesh['sp'=64,'tp'=4] {'sp'}, dimensions={0} | all-to-all | bytes 2097152 | tf_op jit(solution)/shard_map/all_to_all | solution.py:93
  110.8 2.5 collective-permute-start.6
  113.3 22.2 %collective-permute-done.5 = bf16[256,2048]{1,0:T(8,128)(2,1)} collective-permute-done((bf16[256,2048]{1,0:T(8,128)(2,1)S(1)}, bf16[256,2048]{1,0:T(8,128)(2,1)}, u32[]{:S(2)}, u32[]{:S(2)}) %collective-permute-start.5) | collective-permute-done | bytes 1048608 | tf_op jit(solution)/shard_map/ppermute | solution.py:21
  137.5 1.5 constant_dynamic-update-slice_fusion.1
  138.9 20.8 %collective-permute-done.7 = bf16[256,2048]{1,0:T(8,128)(2,1)} collective-permute-done((bf16[256,2048]{1,0:T(8,128)(2,1)}, bf16[256,2048]{1,0:T(8,128)(2,1)}, u32[]{:S(2)}, u32[]{:S(2)}) %collective-permute-start.7) | collective-permute-done | bytes 1048608 | tf_op jit(solution)/shard_map/ppermute | solution.py:21
  161.0 2.0 copy-done.7
  163.0 3.7 fusion.12
  166.7 10.3 %convolution_convert_fusion = bf16[1024,2048]{1,0:T(8,128)(2,1)} fusion(bf16[1,512,2048]{2,1,0:T(8,128)(2,1)S(1)} %copy-done, f32[1024,512]{1,0:T(8,128)} %fusion.12, bf16[1024,2048]{1,0:T(8,128)(2,1)} %copy-done.7, bf16[1,2048,512]{2,1,0:T(8,128)(2,1)} %param.21), kind=kOutput, calls=%fused_computation.1 | convolution fusion | flops 4302307328 | bytes 14680064 | tf_op jit(solution)/shard_map/dot_general | solution.py:98
  178.2 37.1 %all_to_all.26 = bf16[64,4,2048]{2,1,0:T(4,128)(2,1)} all-to-all(bf16[64,4,2048]{2,1,0:T(4,128)(2,1)S(1)} %copy-done.8), channel_id=1, replica_groups=mesh['sp'=64,'tp'=4] {'sp'}, dimensions={0} | all-to-all | bytes 2097152 | tf_op jit(solution)/shard_map/all_to_all | solution.py:93
  216.8 2.7 collective-permute-start.3
  219.4 25.2 %collective-permute-done.2 = bf16[256,2048]{1,0:T(8,128)(2,1)S(1)} collective-permute-done((bf16[256,2048]{1,0:T(8,128)(2,1)S(1)}, bf16[256,2048]{1,0:T(8,128)(2,1)S(1)}, u32[]{:S(2)}, u32[]{:S(2)}) %collective-permute-start.2) | collective-permute-done | bytes 1048608 | tf_op jit(solution)/shard_map/ppermute | solution.py:21
  245.6 24.1 %collective-permute-done.4 = bf16[256,2048]{1,0:T(8,128)(2,1)S(1)} collective-permute-done((bf16[256,2048]{1,0:T(8,128)(2,1)S(1)}, bf16[256,2048]{1,0:T(8,128)(2,1)S(1)}, u32[]{:S(2)}, u32[]{:S(2)}) %collective-permute-start.4) | collective-permute-done | bytes 1048608 | tf_op jit(solution)/shard_map/ppermute | solution.py:21
  269.8 2.0 copy-done.6
  271.8 3.7 fusion.14
  275.4 10.3 %convolution_convert_fusion.1 = bf16[1024,2048]{1,0:T(8,128)(2,1)} fusion(bf16[1,512,2048]{2,1,0:T(8,128)(2,1)S(1)} %copy-done, f32[1024,512]{1,0:T(8,128)} %fusion.14, bf16[1024,2048]{1,0:T(8,128)(2,1)} %copy-done.6, bf16[1,2048,512]{2,1,0:T(8,128)(2,1)} %param.21), kind=kOutput, calls=%fused_computation.2 | convolution fusion | flops 4302307328 | bytes 14680064 | tf_op jit(solution)/shard_map/dot_general | solution.py:98
  285.8 2.2 reshape.56
  288.1 12.0 %all-to-all-start.4 = ((bf16[64,4,2048]{2,1,0:T(4,128)(2,1)}), bf16[64,4,2048]{2,1,0:T(4,128)(2,1)S(1)}, u32[]{:S(2)}, u32[]{:S(2)}) async-start(bf16[64,4,2048]{2,1,0:T(4,128)(2,1)} %reshape.56), calls=%async_computation.6 | async-start | bytes 2097152 | tf_op jit(solution)/shard_map/all_to_all | solution.py:103
  300.1 35.4 %reduce-scatter.3.cloned.1.call-done = bf16[256,2048]{1,0:T(8,128)(2,1)} async-done(((bf16[1024,2048]{1,0:T(8,128)(2,1)}), bf16[256,2048]{1,0:T(8,128)(2,1)}) %reduce-scatter.3.cloned.1.call-update) | async-done | bytes 1048592 | tf_op jit(solution)/shard_map/reduce_scatter | solution.py:99
  335.5 2.2 reshape.54
  338.7 10.7 %all-to-all-start.2 = ((bf16[64,4,2048]{2,1,0:T(4,128)(2,1)}), bf16[64,4,2048]{2,1,0:T(4,128)(2,1)S(1)}, u32[]{:S(2)}, u32[]{:S(2)}) async-start(bf16[64,4,2048]{2,1,0:T(4,128)(2,1)} %reshape.54), calls=%async_computation.3 | async-start | bytes 2097152 | tf_op jit(solution)/shard_map/all_to_all | solution.py:103
  352.0 3.8 convolution_bitcast_fusion.1
  355.8 2.5 convolution_bitcast_fusion
  358.3 19.3 %all-to-all-done.2 = bf16[64,4,2048]{2,1,0:T(4,128)(2,1)S(1)} async-done(((bf16[64,4,2048]{2,1,0:T(4,128)(2,1)}), bf16[64,4,2048]{2,1,0:T(4,128)(2,1)S(1)}, u32[]{:S(2)}, u32[]{:S(2)}) %all-to-all-start.2) | async-done | bytes 1048608 | tf_op jit(solution)/shard_map/all_to_all | solution.py:103
  379.3 3.9 fusion.5
  (75 shorter events, 18.9 us)
Async XLA Ops:
  6.5 160.2 %copy-start = (bf16[1,512,2048]{2,1,0:T(8,128)(2,1)S(1)}, bf16[1,512,2048]{2,1,0:T(8,128)(2,1)}, u32[]{:S(2)}) copy-start(bf16[1,512,2048]{2,1,0:T(8,128)(2,1)} %param.23) | copy-start | bytes 6291460
  6.5 10.9 %copy-start.11 = (bf16[768,256]{1,0:T(8,128)(2,1)S(1)}, bf16[768,256]{1,0:T(8,128)(2,1)}, u32[]{:S(2)}) copy-start(bf16[768,256]{1,0:T(8,128)(2,1)} %param.14) | copy-start | bytes 1179652
  6.5 10.9 %copy-start.9 = (bf16[256,2048]{1,0:T(8,128)(2,1)S(1)}, bf16[256,2048]{1,0:T(8,128)(2,1)}, u32[]{:S(2)}) copy-start(bf16[256,2048]{1,0:T(8,128)(2,1)} %param.16) | copy-start | bytes 3145732
  7.9 7.2 %collective-permute-start = (bf16[1,256]{1,0:T(2,128)(2,1)S(1)}, bf16[1,256]{1,0:T(2,128)(2,1)S(1)}, u32[]{:S(2)}, u32[]{:S(2)}) collective-permute-start(bf16[1,256]{1,0:T(2,128)(2,1)S(1)} %get-tuple-element.11), channel_id=1, source_target_pairs={{0,4},{4,8},{8,12},{12,16},{16,20},{20,24},{24,28},{28,32},{32,36}... | collective-permute-start | bytes 1544 | tf_op jit(solution)/shard_map/ppermute | solution.py:35
  12.4 4.9 %collective-permute-start.1 = (bf16[1,256]{1,0:T(2,128)(2,1)S(1)}, bf16[1,256]{1,0:T(2,128)(2,1)S(1)}, u32[]{:S(2)}, u32[]{:S(2)}) collective-permute-start(bf16[1,256]{1,0:T(2,128)(2,1)S(1)} %get-tuple-element.12), channel_id=1, source_target_pairs={{4,0},{8,4},{12,8},{16,12},{20,16},{24,20},{28,24},{32,28},{36,32}... | collective-permute-start | bytes 1544 | tf_op jit(solution)/shard_map/ppermute | solution.py:36
  20.2 4.8 %copy-start.13 = (s32[192,2]{0,1:T(2,128)S(1)}, s32[192,2]{0,1:T(2,128)}, u32[]{:S(2)}) copy-start(s32[192,2]{0,1:T(2,128)} %param.19) | copy-start | bytes 4612
  20.2 41.3 %all-to-all-start = ((bf16[4,192,2048]{2,1,0:T(8,128)(2,1)}), bf16[4,192,2048]{2,1,0:T(8,128)(2,1)}, u32[]{:S(2)}, u32[]{:S(2)}) async-start(bf16[4,192,2048]{2,1,0:T(8,128)(2,1)} %bitcast.54), calls=%async_computation | async-start | bytes 6291456 | tf_op jit(solution)/shard_map/all_to_all | solution.py:67
  25.0 260.8 %reduce-scatter.5.cloned.1.call-start = ((), (), s32[]{:S(2)}) async-start(), calls=%async_computation.8 | async-start | bytes 5242880 | tf_op jit(solution)/shard_map/reduce_scatter | solution.py:99
  26.0 38.3 %copy-start.10 = (bf16[192,2048]{1,0:T(8,128)(2,1)S(1)}, bf16[192,2048]{1,0:T(8,128)(2,1)}, u32[]{:S(2)}) copy-start(bf16[192,2048]{1,0:T(8,128)(2,1)} %param.17) | copy-start | bytes 2359300
  64.3 1.2 copy-start.12
  64.6 0.9 copy-start.3
  110.5 25.0 %collective-permute-start.5 = (bf16[256,2048]{1,0:T(8,128)(2,1)S(1)}, bf16[256,2048]{1,0:T(8,128)(2,1)}, u32[]{:S(2)}, u32[]{:S(2)}) collective-permute-start(bf16[256,2048]{1,0:T(8,128)(2,1)S(1)} %reshape.55), channel_id=1, source_target_pairs={{0,1},{1,2},{2,3},{3,0},{4,5},{5,6},{6,7},{7,4},{8,9},{9,10},{10,1... | collective-permute-start | bytes 3145736 | tf_op jit(solution)/shard_map/ppermute | solution.py:21
  110.8 26.7 %collective-permute-start.6 = (bf16[256,2048]{1,0:T(8,128)(2,1)S(1)}, bf16[256,2048]{1,0:T(8,128)(2,1)}, u32[]{:S(2)}, u32[]{:S(2)}) collective-permute-start(bf16[256,2048]{1,0:T(8,128)(2,1)S(1)} %reshape.55), channel_id=1, source_target_pairs={{0,3},{1,0},{2,1},{3,2},{4,7},{5,4},{6,5},{7,6},{8,11},{9,8},{10,9... | collective-permute-start | bytes 3145736 | tf_op jit(solution)/shard_map/ppermute | solution.py:24
  135.5 24.2 %collective-permute-start.7 = (bf16[256,2048]{1,0:T(8,128)(2,1)}, bf16[256,2048]{1,0:T(8,128)(2,1)}, u32[]{:S(2)}, u32[]{:S(2)}) collective-permute-start(bf16[256,2048]{1,0:T(8,128)(2,1)} %collective-permute-done.5), channel_id=1, source_target_pairs={{0,1},{1,2},{2,3},{3,0},{4,5},{5,6},{6,7},{7,4},{8,9},{9,10},{10,1... | collective-permute-start | bytes 3145736 | tf_op jit(solution)/shard_map/ppermute | solution.py:21
  137.4 25.6 %copy-start.15 = (bf16[1,2048,512]{2,1,0:T(8,128)(2,1)S(1)}, bf16[1,2048,512]{2,1,0:T(8,128)(2,1)}, u32[]{:S(2)}) copy-start(bf16[1,2048,512]{2,1,0:T(8,128)(2,1)} %param.22) | copy-start | bytes 6291460
  161.0 2.0 copy-start.7
  177.0 1.2 copy-start.8
  177.0 158.5 %reduce-scatter.3.cloned.1.call-start = ((), (), s32[]{:S(2)}) async-start(), calls=%async_computation.7 | async-start | bytes 5242880 | tf_op jit(solution)/shard_map/reduce_scatter | solution.py:99
  216.7 28.0 %collective-permute-start.2 = (bf16[256,2048]{1,0:T(8,128)(2,1)S(1)}, bf16[256,2048]{1,0:T(8,128)(2,1)S(1)}, u32[]{:S(2)}, u32[]{:S(2)}) collective-permute-start(bf16[256,2048]{1,0:T(8,128)(2,1)S(1)} %reshape.53), channel_id=1, source_target_pairs={{0,1},{1,2},{2,3},{3,0},{4,5},{5,6},{6,7},{7,4},{8,9},{9,10},{10,1... | collective-permute-start | bytes 3145736 | tf_op jit(solution)/shard_map/ppermute | solution.py:21
  216.8 28.7 %collective-permute-start.3 = (bf16[256,2048]{1,0:T(8,128)(2,1)S(1)}, bf16[256,2048]{1,0:T(8,128)(2,1)S(1)}, u32[]{:S(2)}, u32[]{:S(2)}) collective-permute-start(bf16[256,2048]{1,0:T(8,128)(2,1)S(1)} %reshape.53), channel_id=1, source_target_pairs={{0,3},{1,0},{2,1},{3,2},{4,7},{5,4},{6,5},{7,6},{8,11},{9,8},{10,9... | collective-permute-start | bytes 3145736 | tf_op jit(solution)/shard_map/ppermute | solution.py:24
  244.6 25.0 %collective-permute-start.4 = (bf16[256,2048]{1,0:T(8,128)(2,1)S(1)}, bf16[256,2048]{1,0:T(8,128)(2,1)S(1)}, u32[]{:S(2)}, u32[]{:S(2)}) collective-permute-start(bf16[256,2048]{1,0:T(8,128)(2,1)S(1)} %collective-permute-done.2), channel_id=1, source_target_pairs={{0,1},{1,2},{2,3},{3,0},{4,5},{5,6},{6,7},{7,4},{8,9},{9,10},{10,1... | collective-permute-start | bytes 3145736 | tf_op jit(solution)/shard_map/ppermute | solution.py:21
  245.4 26.4 %copy-start.16 = (bf16[1,2048,512]{2,1,0:T(8,128)(2,1)S(1)}, bf16[1,2048,512]{2,1,0:T(8,128)(2,1)}, u32[]{:S(2)}) copy-start(bf16[1,2048,512]{2,1,0:T(8,128)(2,1)} %param.22) | copy-start | bytes 6291460
  269.8 2.0 copy-start.6
  288.1 49.7 %all-to-all-start.4 = ((bf16[64,4,2048]{2,1,0:T(4,128)(2,1)}), bf16[64,4,2048]{2,1,0:T(4,128)(2,1)S(1)}, u32[]{:S(2)}, u32[]{:S(2)}) async-start(bf16[64,4,2048]{2,1,0:T(4,128)(2,1)} %reshape.56), calls=%async_computation.6 | async-start | bytes 2097152 | tf_op jit(solution)/shard_map/all_to_all | solution.py:103
  300.1 49.4 %copy-start.14 = (f32[192,2]{0,1:T(2,128)S(1)}, f32[192,2]{0,1:T(2,128)}, u32[]{:S(2)}) copy-start(f32[192,2]{0,1:T(2,128)} %param.20) | copy-start | bytes 4612
  337.7 1.0 copy-start.1
  338.7 38.9 %all-to-all-start.2 = ((bf16[64,4,2048]{2,1,0:T(4,128)(2,1)}), bf16[64,4,2048]{2,1,0:T(4,128)(2,1)S(1)}, u32[]{:S(2)}, u32[]{:S(2)}) async-start(bf16[64,4,2048]{2,1,0:T(4,128)(2,1)} %reshape.54), calls=%async_computation.3 | async-start | bytes 2097152 | tf_op jit(solution)/shard_map/all_to_all | solution.py:103
  350.6 5.2 %copy-start.2 = (bf16[64,4,2048]{2,1,0:T(4,128)(2,1)S(1)}, bf16[64,4,2048]{2,1,0:T(4,128)(2,1)}, u32[]{:S(2)}) copy-start(bf16[64,4,2048]{2,1,0:T(4,128)(2,1)} %copy-done.1) | copy-start | bytes 3145732
  377.6 1.4 copy-start.4
  377.6 1.7 copy-start.5
Sparse Core Ops, SparseCore 0:
  177.2 47.5 reduce-scatter.4
  285.9 49.5 reduce-scatter.2
